TPU v7x, 1024 devices: a whole 4x8x16 slice. The times are simulated.
1024 devices in a mesh: fs: 256 (over z, y, core), tp: 4 (over x).
Axes of the slice: x: 4, y: 8, z: 16, core: 2. Of those that a mesh axis runs over, the one named last changes fastest.
Arguments:
- inputs: bfloat16 [524288, 2048], P('fs'), may hold values from -24 to 24
- key_grads: bfloat16 [524288, 1024], P('fs', 'tp'), may hold values from -0.01953125 to 0.01953125
- weights: float32 [2048, 1024], P('fs', 'tp'), may hold values from -6 to 6
- momentum: float32 [2048, 1024], P('fs', 'tp'), may hold values from -6 to 6
- left_stat: float32 [4, 2048, 2048], P('tp', 'fs'), may hold values from -96 to 96
- right_stat: float32 [8, 128, 128], P('tp'), may hold values from -256 to 256
- left_root: bfloat16 [4, 2048, 2048], P('tp', 'fs'), may hold values from -0.125 to 0.125
- right_root: bfloat16 [8, 128, 128], P('tp'), may hold values from -0.5 to 0.5
Outputs:
- momentum_next: float32 [2048, 1024], P('fs', 'tp')
- left_next: float32 [4, 2048, 2048], P('tp', 'fs')
- right_next: float32 [8, 128, 128], P('tp')
- update: float32 [2048, 1024], P('fs', 'tp')
- weights_next: float32 [2048, 1024], P('fs', 'tp')
- weights_copy: bfloat16 [2048, 1024], P(None, 'tp')
All inputs are finite; a program needn't handle non-finite values.
Results may differ from a plain program's by a relative error of at most 0.0033.
Values may be sent and summed in bfloat16 or wider, within the bound.
A program may use at most 64 MiB of HBM per device.

v0:
```python
import jax
import jax.numpy as jnp
from jax import lax
from jax.sharding import Mesh
from jax.sharding import PartitionSpec as P

FS = ("fs_0", "fs_1", "fs_2")
FS_TP = ("fs_0", "fs_1", "fs_2", "tp")


def by_axis(array, axes):
    for axis in axes:
        array = lax.psum(array, axis)
    return array


def in_order(blocks, dim):
    blocks = jnp.moveaxis(blocks, 0, dim)
    shape = blocks.shape
    return blocks.reshape(*shape[:dim], shape[dim] * shape[dim + 1], *shape[dim + 2 :])


def stacked_from(array, axes, turns):
    blocks = array[None]
    for k in turns:
        blocks = lax.all_gather(blocks, axes[k], axis=0, tiled=True)
    current = [lax.axis_size(axes[k]) for k in reversed(turns)]
    blocks = blocks.reshape(*current, *array.shape)
    turned = sorted(range(len(turns)), key=lambda place: turns[len(turns) - 1 - place])
    return blocks.transpose(*turned, *range(len(turns), blocks.ndim)).reshape(-1, *array.shape)


def whole_of(array, axes, turns, dim):
    return in_order(stacked_from(array, axes, turns), dim)


def body(inputs, key_grads, weights, momentum, left_stat, right_stat, left_root, right_root):
    row_count = weights.shape[0]
    col_count = weights.shape[1]
    block_count = left_root.shape[0]
    head_count = right_root.shape[0]
    head_size = right_root.shape[1]
    model_width = inputs.shape[1]
    partial_grad = lax.dot_general(
        inputs, key_grads, (((0,), (0,)), ((), ())), preferred_element_type=jnp.float32
    )
    summed = lax.psum(partial_grad, FS)
    whole_bf = summed.astype(jnp.bfloat16)
    row_offset = lax.axis_index(FS) * row_count
    grad = lax.dynamic_slice_in_dim(summed, row_offset, row_count, 0)
    own_rows = lax.dynamic_slice_in_dim(whole_bf, row_offset, row_count, 0)
    whole_blocks = whole_bf.reshape(model_width, block_count, -1)
    left_part = jnp.einsum(
        "brd,dbc->rbc", left_root, whole_blocks, preferred_element_type=jnp.float32
    ).reshape(row_count, col_count)
    row_gram = jnp.einsum(
        "rbc,dbc->brd",
        own_rows.reshape(row_count, block_count, -1),
        whole_blocks,
        preferred_element_type=jnp.float32,
    )
    whole_heads = whole_bf.reshape(model_width, head_count, head_size)
    head_gram = jnp.einsum(
        "dhi,dhj->hij", whole_heads, whole_heads, preferred_element_type=jnp.float32
    )
    left_bf = left_part.astype(jnp.bfloat16)
    precond = jnp.einsum(
        "rhi,hij->rhj",
        left_bf.reshape(row_count, head_count, head_size),
        right_root,
        preferred_element_type=jnp.float32,
    ).reshape(row_count, col_count)
    left_next = 0.95 * left_stat + 0.05 * row_gram
    right_next = 0.95 * right_stat + 0.05 * head_gram
    grad_square, precond_square = (
        by_axis(jnp.sum(grad * grad), FS_TP),
        by_axis(jnp.sum(precond * precond), FS_TP),
    )
    scale = jnp.sqrt(grad_square / (precond_square + 1e-06))
    momentum_next = 0.9 * momentum + scale * precond
    update = -0.25 * (momentum_next + 0.4 * weights)
    weights_next = weights + update
    weights_copy = whole_of(weights_next.astype(jnp.bfloat16), FS, (0, 1, 2), 0)
    return (momentum_next, left_next, right_next, update, weights_next, weights_copy)


def solution(mesh):
    split = Mesh(mesh.devices.reshape(16, 8, 2, mesh.shape["tp"]), ("fs_0", "fs_1", "fs_2", "tp"))
    in_specs = (
        P(FS, None),
        P(FS, "tp"),
        P(FS, "tp"),
        P(FS, "tp"),
        P("tp", FS, None),
        P("tp", None, None),
        P("tp", FS, None),
        P("tp", None, None),
    )
    out_specs = (
        P(FS, "tp"),
        P("tp", FS, None),
        P("tp", None, None),
        P(FS, "tp"),
        P(FS, "tp"),
        P(None, "tp"),
    )
    return jax.shard_map(body, mesh=split, in_specs=in_specs, out_specs=out_specs, check_vma=False)
```

profile of v0, /device:TPU:1, one launch (start us, length us, event | category | flops | bytes accessed | tf_op | source)
XLA Modules:
  0.0 533.9 jit_solution(7610762753888100599)
XLA Ops:
  7.2 0.0 copy-start
  7.2 0.0 all-reduce.6.cloned.1.call-start
  7.2 1.2 copy-done
  8.4 7.1 %fusion.14 = f32[2048,256]{1,0:T(8,128)} fusion(bf16[2048,2048]{1,0:T(8,128)(2,1)} %param.8, bf16[2048,256]{1,0:T(8,128)(2,1)S(1)} %copy-done), kind=kOutput, calls=%fused_computation.18 | convolution fusion | flops 2147483648 | bytes 11534336 | tf_op jit(solution)/shard_map/dot_general | solution.py:44
  15.5 0.0 all-reduce.6.cloned.1.call-update
  15.6 0.0 copy-start.2
  15.6 0.0 copy-start.4
  15.6 0.0 all-gather.3.cloned.1.call-start
  15.7 0.0 copy-start.5
  15.7 0.0 copy-start.6
  15.7 0.0 copy-start.3
  15.7 369.9 %all-reduce.6.cloned.1.call-done = f32[2048,256]{1,0:T(8,128)} async-done(((f32[2048,256]{1,0:T(8,128)}), f32[2048,256]{1,0:T(8,128)}) %all-reduce.6.cloned.1.call-update) | async-done | bytes 2097168 | tf_op jit(solution)/shard_map/psum | solution.py:47
  385.6 1.7 convert_element_type.19
  387.3 0.0 copy-done.2
  387.3 0.0 copy-done.4
  387.3 0.0 copy-start.1
  387.3 1.0 multiply_reduce_fusion
  388.3 1.3 multiply_reduce_fusion.1
  389.6 22.7 %all-reduce = (f32[]{:T(128)}, f32[]{:T(128)}) all-reduce(f32[]{:T(128)} %multiply_reduce_fusion.1, f32[]{:T(128)} %get-tuple-element.18), channel_id=1, replica_groups=mesh['fs_0'=16,'fs_1'=8,'fs_2'=2,'tp'=4] {'fs_0'}, use_global_device_ids=true, to_apply=%region_2.0 | all-reduce | flops 2 | bytes 16 | tf_op jit(solution)/shard_map/psum | solution.py:13
  412.3 13.2 %all-reduce.1 = (f32[]{:T(128)}, f32[]{:T(128)}) all-reduce(f32[]{:T(128)} %get-tuple-element.6, f32[]{:T(128)} %get-tuple-element.7), channel_id=1, replica_groups=mesh['fs_0'=16,'fs_1'=8,'fs_2'=2,'tp'=4] {'fs_1'}, use_global_device_ids=true, to_apply=%region_3.0 | all-reduce | flops 2 | bytes 16 | tf_op jit(solution)/shard_map/psum | solution.py:13
  425.4 13.5 %all-reduce.3 = (f32[]{:T(128)}, f32[]{:T(128)}) all-reduce(f32[]{:T(128)} %get-tuple-element.8, f32[]{:T(128)} %get-tuple-element.9), channel_id=1, replica_groups=mesh['fs_0'=16,'fs_1'=8,'fs_2'=2,'tp'=4] {'fs_2'}, use_global_device_ids=true, to_apply=%region_4.0 | all-reduce | flops 2 | bytes 16 | tf_op jit(solution)/shard_map/psum | solution.py:13
  439.0 9.0 %all-reduce.2 = (f32[]{:T(128)}, f32[]{:T(128)}) all-reduce(f32[]{:T(128)} %get-tuple-element.12, f32[]{:T(128)} %get-tuple-element.13), channel_id=1, replica_groups=mesh['fs_0'=16,'fs_1'=8,'fs_2'=2,'tp'=4] {'tp'}, use_global_device_ids=true, to_apply=%region_5.0 | all-reduce | flops 2 | bytes 16 | tf_op jit(solution)/shard_map/psum | solution.py:13
  449.3 0.0 copy-done.5
  449.3 0.0 copy-done.6
  449.3 0.6 fusion.11
  450.0 20.2 %all-gather = bf16[128,256]{1,0:T(8,128)(2,1)S(1)} all-gather(bf16[8,256]{1,0:T(8,128)(2,1)S(1)} %get-tuple-element.14), channel_id=2, replica_groups=mesh['fs_0'=16,'fs_1'=8,'fs_2'=2,'tp'=4] {'fs_0'}, dimensions={0}, use_global_device_ids=true | all-gather | bytes 69632 | tf_op jit(solution)/shard_map/all_gather | solution.py:26
  470.2 21.9 %all_gather.10 = bf16[128,8,256]{2,1,0:T(8,128)(2,1)} all-gather(bf16[16,8,256]{2,1,0:T(8,128)(2,1)S(1)} %bitcast.44), channel_id=1, replica_groups=mesh['fs_0'=16,'fs_1'=8,'fs_2'=2,'tp'=4] {'fs_1'}, dimensions={0}, use_global_device_ids=true | all-gather | bytes 589824 | tf_op jit(solution)/shard_map/all_gather | solution.py:26
  492.1 0.0 all-gather.3.cloned.1.call-update
  492.1 0.0 copy-done.3
  492.1 1.0 fusion.1
  493.1 0.0 copy-done.1
  493.1 3.4 fusion.2
  496.5 28.3 %all-gather.3.cloned.1.call-done = bf16[256,8,256]{2,1,0:T(8,128)(2,1)} async-done(((bf16[128,8,256]{2,1,0:T(8,128)(2,1)}), bf16[256,8,256]{2,1,0:T(8,128)(2,1)}) %all-gather.3.cloned.1.call-update) | async-done | bytes 1048592 | tf_op jit(solution)/shard_map/all_gather | solution.py:26
  524.8 2.3 copy.23
Async XLA Ops:
  7.2 1.2 copy-start
  7.2 378.4 %all-reduce.6.cloned.1.call-start = ((), (), s32[]{:S(2)}) async-start(), calls=%async_computation | async-start | bytes 4194304 | tf_op jit(solution)/shard_map/psum | solution.py:47
  15.6 371.7 %copy-start.2 = (bf16[2,128,128]{2,1,0:T(8,128)(2,1)S(1)}, bf16[2,128,128]{2,1,0:T(8,128)(2,1)}, u32[]{:S(2)}) copy-start(bf16[2,128,128]{2,1,0:T(8,128)(2,1)} %param.15) | copy-start | bytes 196612
  15.6 371.7 %copy-start.4 = (bf16[1,8,2048]{2,1,0:T(8,128)(2,1)S(1)}, bf16[1,8,2048]{2,1,0:T(8,128)(2,1)}, u32[]{:S(2)}) copy-start(bf16[1,8,2048]{2,1,0:T(8,128)(2,1)} %param.14) | copy-start | bytes 98308
  15.6 509.2 %all-gather.3.cloned.1.call-start = ((), (), s32[]{:S(2)}) async-start(), calls=%async_computation.1 | async-start | bytes 1572864 | tf_op jit(solution)/shard_map/all_gather | solution.py:26
  15.7 433.7 %copy-start.5 = (f32[8,256]{1,0:T(8,128)S(1)}, f32[8,256]{1,0:T(8,128)}, u32[]{:S(2)}) copy-start(f32[8,256]{1,0:T(8,128)} %param.10) | copy-start | bytes 24580
  15.7 433.7 %copy-start.6 = (f32[8,256]{1,0:T(8,128)S(1)}, f32[8,256]{1,0:T(8,128)}, u32[]{:S(2)}) copy-start(f32[8,256]{1,0:T(8,128)} %param.11) | copy-start | bytes 24580
  15.7 476.4 %copy-start.3 = (f32[1,8,2048]{2,1,0:T(8,128)S(1)}, f32[1,8,2048]{2,1,0:T(8,128)}, u32[]{:S(2)}) copy-start(f32[1,8,2048]{2,1,0:T(8,128)} %param.12) | copy-start | bytes 196612
  387.3 105.9 %copy-start.1 = (f32[2,128,128]{2,1,0:T(8,128)S(1)}, f32[2,128,128]{2,1,0:T(8,128)}, u32[]{:S(2)}) copy-start(f32[2,128,128]{2,1,0:T(8,128)} %param.13) | copy-start | bytes 393220
Sparse Core Ops, SparseCore 0:
  15.7 369.8 all-reduce.5
  492.2 32.5 all-gather.2
where the time goes:
time: 534 us
  waiting for transfers between devices  398 us (75%)
  blocking collectives  100 us (19%)
  between operations  15.5 us (3%)
  matrix products  12.5 us (2%)
    psum x1, waiting for transfers between devices, body(): summed = lax.psum(partial_grad, FS)  370 us
    psum x4, blocking collectives, by_axis(): array = lax.psum(array, axis)  58.4 us
    all_gather x2, blocking collectives, stacked_from(): blocks = lax.all_gather(blocks, axes[k], axis=0, tiled=True)  42.1 us
    all_gather x1, waiting for transfers between devices, stacked_from(): blocks = lax.all_gather(blocks, axes[k], axis=0, tiled=True)  28.3 us
  transfers between devices with their start and end apart: 2, of which 2 were waited for; matrix products, arithmetic and copies ran while one was open for 1% of the time, Pallas kernels for 0%

commit v1 on v0

v1 whole, which is shorter than its diff:
```python
import functools

import jax
import jax.numpy as jnp
from jax import lax
from jax.experimental import pallas as pl
from jax.experimental.pallas import tpu as pltpu
from jax.sharding import Mesh
from jax.sharding import PartitionSpec as P

MESH = pl.DeviceIdType.MESH
F32 = jnp.float32
BF16 = jnp.bfloat16
H = 128
ROWS = 16


def offset_of(r, nz):
    half = nz // 2
    if r == 0:
        return half
    return half - (r + 1) // 2 if r % 2 else -(half - r // 2)


def place_of(off, nz):
    half = nz // 2
    if off == 0:
        return nz - 1
    if abs(off) == half:
        return 0
    return 2 * (half - off) - 1 if off > 0 else 2 * (half + off)


def kernel(
    nz, ny, nx, gz,
    x_hbm, k_hbm, w_hbm, m_hbm, ls_hbm, rs_hbm, lr_hbm, rr_hbm,
    mom_hbm, ln_hbm, rn_hbm, up_hbm, wn_hbm, cp_hbm,
    xs, ks, kt, pt, px, sf, ysend, yrecv, zsend, zrecv, gfull, gabs, pfull, afull, ascr, tile, own8, gown,
    wv, mv, lsv, rsv, lrv, rrv, momv, lnv, rnv, upv, wnv, outv,
    sv, s1, s2, s3,
    in_sem, x_sem, out_sem, d_send, d_recv, ry_send, ry_recv, rz_sem, a_sem, ring_send, ring_r, ring_l,
    ag_send, agz_recv, agy_recv, agd_recv, s_send, s_recv,
):
    ng = nz // gz
    blk = ny * ROWS
    z, y, c, x = (lax.axis_index(n) for n in ("z", "y", "c", "x"))
    me = nz - 1
    other = 1 - c
    partner = {"c": other}

    def zpos(off):
        return lax.rem(z + off + nz, nz)

    def ypos(dy):
        return lax.rem(y + dy, ny)

    def send(src, dst, s, r, dev):
        pltpu.make_async_remote_copy(src, dst, s, r, device_id=dev, device_id_type=MESH).start()

    def await_bytes(ref, sem):
        pltpu.make_async_copy(ref, ref, sem).wait()

    xc_peers = [(dx, dc) for dx in range(nx) for dc in range(2) if dx or dc]

    def xc_dev(dx, dc):
        return {"x": lax.rem(x + dx, nx), "c": lax.rem(c + dc, 2)}

    bar = pltpu.get_barrier_semaphore()

    @pl.loop(1, ny)
    def _(dy):
        pl.semaphore_signal(bar, inc=1, device_id={"y": ypos(dy)}, device_id_type=MESH)

    @pl.loop(1, nz)
    def _(dz):
        pl.semaphore_signal(bar, inc=1, device_id={"z": lax.rem(z + dz, nz)}, device_id_type=MESH)

    for dx, dc in xc_peers:
        pl.semaphore_signal(bar, inc=1, device_id=xc_dev(dx, dc), device_id_type=MESH)

    def load(src, dst, i):
        pltpu.make_async_copy(src, dst, in_sem.at[i]).start()

    def loaded(dst, i):
        await_bytes(dst, in_sem.at[i])

    load(k_hbm, ks, 0)
    for r in range(nz):
        src = x_hbm.at[:, pl.ds(pl.multiple_of(zpos(offset_of(r, nz)) * blk, blk), blk)]
        pltpu.make_async_copy(src, xs.at[r // gz, :, pl.ds((r % gz) * blk, blk)], x_sem.at[r // gz]).start()
    load(w_hbm, wv, 1)
    load(m_hbm, mv, 2)
    load(lr_hbm.at[0], lrv.at[c], 3)
    load(rr_hbm, rrv, 4)
    load(ls_hbm.at[0], lsv, 5)
    load(rs_hbm, rsv, 6)

    loaded(ks, 0)
    kt[...] = ks[...].T
    for g in range(ng):
        await_bytes(xs.at[g], x_sem.at[g])
        out = jnp.dot(kt[...], xs[g], preferred_element_type=F32)
        for i in range(gz):
            for h in range(2):
                pt[g, h, i] = out[h * H:(h + 1) * H, i * blk:(i + 1) * blk]

    loaded(wv, 1)
    loaded(mv, 2)
    base = 0.9 * wv[...] - 0.225 * mv[...]
    ascr[0] = base[:, :H]
    ascr[1] = base[:, H:]
    afull[c, me, y, pl.ds(pl.multiple_of(8 * c, 8), 8)] = ascr[c]
    loaded(lrv.at[c], 3)

    pl.semaphore_wait(bar, (ny - 1) + (nz - 1) + len(xc_peers))

    for g in range(ng):
        send(pt.at[g, other], px.at[g], d_send.at[0], d_recv.at[g], partner)
    send(ascr.at[other], afull.at[other, me, y, pl.ds(pl.multiple_of(8 * c, 8), 8)], d_send.at[1], d_recv.at[ng], partner)
    send(lrv.at[c], lrv.at[c], d_send.at[2], d_recv.at[ng + 1], partner)

    for g in range(ng):
        await_bytes(px.at[g], d_recv.at[g])
        for i in range(gz):
            r = g * gz + i
            t = (pt[g, c, i] + px[g, i]).T.reshape(ny, ROWS, H)
            sf[r] = t
            ysend[:, r] = t.astype(BF16)

        @pl.loop(1, ny)
        def _(dy):
            yt = ypos(dy)
            send(ysend.at[yt, pl.ds(g * gz, gz)], yrecv.at[dy - 1, pl.ds(g * gz, gz)], ry_send, ry_recv.at[g], {"y": yt})

        if g == 0:
            await_bytes(ascr.at[0], d_recv.at[ng])

            @pl.loop(1, ny)
            def _(dy):
                send(afull.at[c, me, y], afull.at[c, me, y], a_sem.at[0], a_sem.at[1], {"y": ypos(dy)})

    half = nz // 2

    def ring_step(k):
        if k == 1:
            await_bytes(afull.at[c, me, pl.ds(0, ny - 1)], a_sem.at[1])
        else:
            await_bytes(afull.at[c, 0], ring_r.at[k - 2])
            if k <= half:
                await_bytes(afull.at[c, 0], ring_l.at[k - 2])
        if k <= half:
            src, dst = place_of(-(k - 1), nz), place_of(-k, nz)
            send(afull.at[c, src], afull.at[c, dst], ring_send.at[0], ring_r.at[k - 1], {"z": zpos(1)})
        if k < half:
            src, dst = place_of(k - 1, nz), place_of(k, nz)
            send(afull.at[c, src], afull.at[c, dst], ring_send.at[1], ring_l.at[k - 1], {"z": zpos(-1)})

    steps = iter(range(1, half + 2))

    def ring(n):
        for _ in range(n):
            k = next(steps, None)
            if k is None:
                return
            if k == half + 1:
                await_bytes(afull.at[c, 0], ring_r.at[half - 1])
                send(afull.at[c], afull.at[c], d_send.at[3], d_recv.at[ng + 2], partner)
            else:
                ring_step(k)

    ring(1)
    for g in range(ng):
        await_bytes(yrecv.at[:, pl.ds(g * gz, gz)], ry_recv.at[g])
        for i in range(gz):
            r = g * gz + i
            t = sf[r, y]
            for j in range(ny - 1):
                t = t + yrecv[j, r].astype(F32)
            zsend[r] = t
            if r != me:
                off = offset_of(r, nz)
                back = place_of(-off, nz)
                send(zsend.at[r], zrecv.at[back], rz_sem.at[0], rz_sem.at[1], {"z": zpos(off)})
        if g in (1, 3):
            ring(1)

    await_bytes(zrecv, rz_sem.at[1])
    grad = zsend[me]
    for r in range(nz - 1):
        grad = grad + zrecv[r]
    sv[0:1] = jnp.sum(grad * grad, axis=0, keepdims=True)
    gfull[c, me, y] = grad.astype(BF16)

    groups = [(me, 1)] + [(r, 2) for r in range(nz - 3, 0, -2)] + [(0, 1)]

    def gather_start(full, p):
        for r in range(nz - 1):
            off = offset_of(r, nz)
            back = place_of(-off, nz)
            j = [q for q, (r0, n) in enumerate(groups) if r0 <= back < r0 + n][0]
            send(full.at[c, me, y], full.at[c, back, y], ag_send.at[p, 0], agz_recv.at[p, j], {"z": zpos(off)})
        gather_forward(full, p, 0)

    def gather_forward(full, p, j):
        r0, n = groups[j]
        if j:
            await_bytes(full.at[c, pl.ds(r0, n), y], agz_recv.at[p, j])

        @pl.loop(1, ny)
        def _(dy):
            slab = full.at[c, pl.ds(r0, n), y]
            send(slab, slab, ag_send.at[p, 1], agy_recv.at[p, j], {"y": ypos(dy)})

    def gather_land(full, p, j):
        r0, n = groups[j]
        await_bytes(full.at[c, pl.ds(r0, n), pl.ds(0, ny - 1)], agy_recv.at[p, j])
        slab = full.at[c, pl.ds(r0, n)]
        send(slab, slab, ag_send.at[p, 2], agd_recv.at[p, j], partner)

    def gather_close(full, p):
        await_bytes(full.at[0, pl.ds(0, nz - 1), 0], ag_send.at[p, 0])
        await_bytes(full.at[0, :, pl.ds(0, ny - 1)], ag_send.at[p, 1])
        await_bytes(full.at[0], ag_send.at[p, 2])

    gather_start(gfull, 0)
    ring(1)
    for j in range(1, len(groups)):
        gather_forward(gfull, 0, j)
    ring(1)

    def keep(h, j):
        r0, n = groups[j]
        for r in range(r0, r0 + n):
            gabs[h, pl.ds(pl.multiple_of(zpos(offset_of(r, nz)) * blk, blk), blk)] = gfull[h, r].reshape(blk, H)

    for j in range(len(groups)):
        gather_land(gfull, 0, j)
        keep(c, j)

    await_bytes(lrv.at[0], d_recv.at[ng + 1])
    loaded(rrv, 4)
    lm = jnp.concatenate([lrv[0].astype(F32), lrv[1].astype(F32)], axis=0).astype(BF16)
    left = jnp.dot(lm, gabs[c], preferred_element_type=F32)
    hi = left.astype(BF16)
    lo = (left - hi.astype(F32)).astype(BF16)
    rr = rrv[c]
    pre = jnp.dot(hi, rr, preferred_element_type=F32) + jnp.dot(lo, rr, preferred_element_type=F32)
    pfull[c, me, y] = pre.astype(BF16)
    gather_start(pfull, 1)
    sv[1:2] = jnp.sum(pre * pre, axis=0, keepdims=True)
    tile[...] = pre

    s1[x * 2 + c] = sv[...]
    for dx, dc in xc_peers:
        send(sv, s1.at[x * 2 + c], s_send.at[0], s_recv.at[0], xc_dev(dx, dc))
    send(tile.at[pl.ds(pl.multiple_of(8 * other, 8), 8)], own8.at[c], d_send.at[4], d_recv.at[ng + 3], partner)
    own8[c] = tile[pl.ds(pl.multiple_of(8 * c, 8), 8)]
    ring(1)

    for j in range(len(groups)):
        r0, n = groups[j]
        await_bytes(gfull.at[other, pl.ds(r0, n)], agd_recv.at[0, j])
        keep(other, j)
    gram = None
    for h in range(2):
        gown[...] = gfull[h, me, y].astype(F32)
        mine = gown[pl.ds(pl.multiple_of(8 * c, 8), 8)].astype(BF16)
        part = lax.dot_general(mine, gabs[h], (((1,), (1,)), ((), ())), preferred_element_type=F32)
        gram = part if gram is None else gram + part
    loaded(lsv, 5)
    lnv[...] = 0.95 * lsv[...] + 0.05 * gram
    pltpu.make_async_copy(lnv, ln_hbm.at[0], out_sem.at[0]).start()

    await_bytes(s1.at[pl.ds(0, 2 * nx - 1)], s_recv.at[0])
    tot = s1[0]
    for i in range(1, 2 * nx):
        tot = tot + s1[i]
    s2[z] = tot

    @pl.loop(1, nz)
    def _(dz):
        send(s2.at[z], s2.at[z], s_send.at[1], s_recv.at[1], {"z": lax.rem(z + dz, nz)})

    for j in range(1, len(groups)):
        gather_forward(pfull, 1, j)

    loaded(rsv, 6)
    for h in range(2):
        gh = gabs[h]
        hg = lax.dot_general(gh, gh, (((0,), (0,)), ((), ())), preferred_element_type=F32)
        rnv[h] = 0.95 * rsv[h] + 0.05 * hg
    pltpu.make_async_copy(rnv, rn_hbm, out_sem.at[1]).start()

    await_bytes(s2.at[pl.ds(0, nz - 1)], s_recv.at[1])
    tot = s2[0]
    for i in range(1, nz):
        tot = tot + s2[i]
    s3[y] = tot

    @pl.loop(1, ny)
    def _(dy):
        send(s3.at[y], s3.at[y], s_send.at[2], s_recv.at[2], {"y": ypos(dy)})

    ring(nz)
    for j in range(len(groups)):
        gather_land(pfull, 1, j)

    await_bytes(s3.at[pl.ds(0, ny - 1)], s_recv.at[2])
    tot = s3[0]
    for i in range(1, ny):
        tot = tot + s3[i]
    gs = jnp.sum(tot[0:1], axis=1, keepdims=True)
    ps = jnp.sum(tot[1:2], axis=1, keepdims=True)
    scale = jnp.sqrt(gs / (ps + 1e-06))

    await_bytes(own8.at[0], d_recv.at[ng + 3])
    wide = jnp.concatenate([own8[0], own8[1]], axis=1)
    mom = 0.9 * mv[...] + scale * wide
    upd = -0.25 * (mom + 0.4 * wv[...])
    momv[...] = mom
    upv[...] = upd
    wnv[...] = wv[...] + upd
    pltpu.make_async_copy(momv, mom_hbm, out_sem.at[2]).start()
    pltpu.make_async_copy(upv, up_hbm, out_sem.at[3]).start()
    pltpu.make_async_copy(wnv, wn_hbm, out_sem.at[4]).start()

    await_bytes(afull.at[other], d_recv.at[ng + 2])
    quarter = 0.25 * scale
    for j in range(len(groups)):
        r0, n = groups[j]
        await_bytes(pfull.at[other, pl.ds(r0, n)], agd_recv.at[1, j])
        for r in range(r0, r0 + n):
            for h in range(2):
                v = afull[h, r].reshape(blk, H) - quarter * pfull[h, r].reshape(blk, H).astype(F32)
                outv[r, :, h * H:(h + 1) * H] = v.astype(BF16)
            dst = cp_hbm.at[pl.ds(pl.multiple_of(zpos(offset_of(r, nz)) * blk, blk), blk)]
            pltpu.make_async_copy(outv.at[r], dst, out_sem.at[5]).start()

    await_bytes(pt.at[:, 0], d_send.at[0])
    await_bytes(ascr.at[0], d_send.at[1])
    await_bytes(lrv.at[0], d_send.at[2])
    await_bytes(afull.at[0], d_send.at[3])
    await_bytes(own8.at[0], d_send.at[4])
    await_bytes(yrecv, ry_send)
    await_bytes(zrecv, rz_sem.at[0])
    await_bytes(afull.at[0, 0, pl.ds(0, ny - 1)], a_sem.at[0])
    await_bytes(afull.at[0, pl.ds(0, half)], ring_send.at[0])
    if half > 1:
        await_bytes(afull.at[0, pl.ds(0, half - 1)], ring_send.at[1])
    gather_close(gfull, 0)
    gather_close(pfull, 1)
    await_bytes(s1.at[pl.ds(0, 2 * nx - 1)], s_send.at[0])
    await_bytes(s2.at[pl.ds(0, nz - 1)], s_send.at[1])
    await_bytes(s3.at[pl.ds(0, ny - 1)], s_send.at[2])
    await_bytes(lnv, out_sem.at[0])
    await_bytes(rnv, out_sem.at[1])
    await_bytes(momv, out_sem.at[2])
    await_bytes(upv, out_sem.at[3])
    await_bytes(wnv, out_sem.at[4])
    await_bytes(outv, out_sem.at[5])


def body(nz, ny, nx, gz, inputs, key_grads, weights, momentum, left_stat, right_stat, left_root, right_root):
    tokens, width = inputs.shape
    ng, blk, ngr = nz // gz, ny * ROWS, nz // 2 + 1
    dma = pltpu.SemaphoreType.DMA
    v = pltpu.VMEM
    scratch = [
        v((ng, tokens, gz * blk), BF16), v((tokens, 2 * H), BF16), v((2 * H, tokens), BF16),
        v((ng, 2, gz, H, blk), F32), v((ng, gz, H, blk), F32),
        v((nz, ny, ROWS, H), F32), v((ny, nz, ROWS, H), BF16), v((ny - 1, nz, ROWS, H), BF16),
        v((nz, ROWS, H), F32), v((nz - 1, ROWS, H), F32),
        v((2, nz, ny, ROWS, H), BF16), v((2, width, H), BF16), v((2, nz, ny, ROWS, H), BF16), v((2, nz, ny, ROWS, H), F32),
        v((2, 8, H), F32), v((ROWS, H), F32), v((2, 8, H), F32), v((ROWS, H), F32),
        v((8, 2 * H), F32), v((8, 2 * H), F32), v((8, width), F32), v((2, H, H), F32), v((2, 8, width), BF16), v((2, H, H), BF16),
        v((8, 2 * H), F32), v((8, width), F32), v((2, H, H), F32), v((8, 2 * H), F32), v((8, 2 * H), F32),
        v((nz, blk, 2 * H), BF16),
        v((2, H), F32), v((2 * nx, 2, H), F32), v((nz, 2, H), F32), v((ny, 2, H), F32),
        dma((7,)), dma((ng,)), dma((6,)), dma((5,)), dma((ng + 4,)), dma, dma((ng,)), dma((2,)), dma((2,)),
        dma((2,)), dma((nz // 2,)), dma((nz // 2,)),
        dma((2, 3)), dma((2, ngr)), dma((2, ngr)), dma((2, ngr)), dma((3,)), dma((3,)),
    ]
    sds = jax.ShapeDtypeStruct
    anyspace = pl.BlockSpec(memory_space=pl.ANY)
    return pl.pallas_call(
        functools.partial(kernel, nz, ny, nx, gz),
        out_shape=(
            sds(weights.shape, F32), sds(left_stat.shape, F32), sds(right_stat.shape, F32),
            sds(weights.shape, F32), sds(weights.shape, F32), sds((width, 2 * H), BF16),
        ),
        in_specs=[anyspace] * 8,
        out_specs=(anyspace,) * 6,
        scratch_shapes=scratch,
        compiler_params=pltpu.CompilerParams(collective_id=0, has_side_effects=True, vmem_limit_bytes=56 * 2**20),
    )(inputs, key_grads, weights, momentum, left_stat, right_stat, left_root, right_root)


def build(devices, nz, ny, nx, gz):
    split = Mesh(devices.reshape(nz, ny, 2, nx), ("z", "y", "c", "x"))
    fs = ("z", "y", "c")
    in_specs = (
        P(fs, None), P(fs, "x"), P(fs, "x"), P(fs, "x"),
        P("x", fs, None), P("x", None, None), P("x", fs, None), P("x", None, None),
    )
    out_specs = (P(fs, "x"), P("x", fs, None), P("x", None, None), P(fs, "x"), P(fs, "x"), P(None, "x"))
    return jax.shard_map(
        functools.partial(body, nz, ny, nx, gz), mesh=split, in_specs=in_specs, out_specs=out_specs, check_vma=False
    )


def solution(mesh):
    return build(mesh.devices, 16, 8, mesh.shape["tp"], 4)
```

time: 534 us -> 96.7 us (0.18)
  waiting for transfers between devices: 398 us -> 0 us
  blocking collectives: 100 us -> 0 us
  Pallas kernels: 0 us -> 86.4 us
  between operations: 15.5 us -> 0.65 us
  matrix products: 12.5 us -> 0 us
  local copies, waits for them, and re-layouts: 3.51 us -> 9.19 us
    psum x1 -> x0, waiting for transfers between devices: 370 us -> none  [body(): summed = lax.psum(partial_grad, FS)]
    pallas_call x0 -> x1, Pallas kernels: none -> 86.4 us  [body(): pl.pallas_call(functools.partial(kernel, nz, ny, nx, gz), out_shape=(sds(...]
    psum x4 -> x0, blocking collectives: 58.4 us -> none  [by_axis(): array = lax.psum(array, axis)]
    all_gather x2 -> x0, blocking collectives: 42.1 us -> none  [stacked_from(): blocks = lax.all_gather(blocks, axes[k], axis=0, tiled=True)]
    all_gather x1 -> x0, waiting for transfers between devices: 28.3 us -> none  [stacked_from(): blocks = lax.all_gather(blocks, axes[k], axis=0, tiled=True)]
    dot_general x4 -> x0, matrix products: 12.5 us -> none  [the longest x1 7.15 us: body(): lax.dot_general(inputs, key_grads, (((0,), (0,)), ((), ())), preferred_el...]
    unnamed x14 -> x6, local copies, waits for them, and re-layouts: 1.22 us -> 9.19 us
  transfers between devices with their start and end apart: 2 -> 0, of which waited for: 2 -> 0; matrix products, arithmetic and copies ran while one was open for 1% -> 0% of each run, Pallas kernels for 0% -> 0%
where the time goes in v1:
time: 96.7 us; the launch traced here: 96.3 us
  Pallas kernels  86.4 us (89%)
  local copies, waits for them, and re-layouts  9.19 us (10%)
    pallas_call x1, Pallas kernels, body(): pl.pallas_call(functools.partial(kernel, nz, ny, nx, gz), out_shape=(sds(...  86.4 us
    unnamed x6, local copies, waits for them, and re-layouts  9.19 us

profile of v1, /device:TPU:1, one launch (start us, length us, event | category | flops | bytes accessed | tf_op | source)
XLA Modules:
  0.0 96.3 jit_solution(17600663005582897359)
XLA Ops:
  0.6 86.4 %shard_map.127 = (f32[8,256]{1,0:T(8,128)}, f32[1,8,2048]{2,1,0:T(8,128)}, f32[2,128,128]{2,1,0:T(8,128)}, f32[8,256]{1,0:T(8,128)}, f32[8,256]{1,0:T(8,128)}, /*index=5*/bf16[2048,256]{1,0:T(8,128)(2,1)}) custom-call(bf16[2048,2048]{1,0:T(8,128)(2,1)} %x_hbm.1, bf16[2048,256]{1,0:T(8,128)(2,1)} %k_hbm.1, f32[8,256]{1,0:T(8,128)} %w_hbm.1, f32[8,256]{1,0:T(8,128)} %m_hbm.1, ...), custom_call_target="tpu_custom_call" | custom-call | tf_op jit(solution)/shard_map/pallas_call | solution.py:385
  87.1 1.3 %copy.20 = f32[8,256]{1,0:T(8,128)} copy(f32[8,256]{1,0:T(8,128)} %get-tuple-element.12) | data formatting | bytes 16384
  88.4 1.5 %copy.21 = f32[1,8,2048]{2,1,0:T(8,128)} copy(f32[1,8,2048]{2,1,0:T(8,128)} %get-tuple-element.13) | data formatting | bytes 131072
  89.9 1.6 %copy.22 = f32[2,128,128]{2,1,0:T(8,128)} copy(f32[2,128,128]{2,1,0:T(8,128)} %get-tuple-element.14) | data formatting | bytes 262144
  91.4 1.3 %copy.23 = f32[8,256]{1,0:T(8,128)} copy(f32[8,256]{1,0:T(8,128)} %get-tuple-element.15) | data formatting | bytes 16384
  92.7 1.3 %copy.24 = f32[8,256]{1,0:T(8,128)} copy(f32[8,256]{1,0:T(8,128)} %get-tuple-element.16) | data formatting | bytes 16384
  94.0 2.3 %copy.25 = bf16[2048,256]{1,0:T(8,128)(2,1)} copy(bf16[2048,256]{1,0:T(8,128)(2,1)} %get-tuple-element.17) | data formatting | bytes 2097152

commit v2 on v1

v2 whole, which is shorter than its diff:
```python
import functools

import jax
import jax.numpy as jnp
from jax import lax
from jax.experimental import pallas as pl
from jax.experimental.pallas import tpu as pltpu
from jax.sharding import Mesh
from jax.sharding import PartitionSpec as P

MESH = pl.DeviceIdType.MESH
F32 = jnp.float32
BF16 = jnp.bfloat16
H = 128
ROWS = 16


def offset_of(r, nz):
    half = nz // 2
    if r == 0:
        return half
    return half - (r + 1) // 2 if r % 2 else -(half - r // 2)


def place_of(off, nz):
    half = nz // 2
    if off == 0:
        return nz - 1
    if abs(off) == half:
        return 0
    return 2 * (half - off) - 1 if off > 0 else 2 * (half + off)


HELD = pltpu.VMEM


def kernel(
    nz, ny, nx, gz,
    x_hbm, k_hbm, w_hbm, m_hbm, ls_hbm, rs_hbm, lr_hbm, rr_hbm,
    momv, lnv, rnv, upv, wnv, outv,
    xs, ks, kt, pt, px, sf, ysend, yrel, ysum, yrecv, zsend, zrecv, gfull, gabs, pfull, afull, ascr, tile, own8, gown,
    wv, mv, lsv, rsv, lrv, rrv,
    sv, s1, s2, s3,
    in_sem, x_sem, d_send, d_recv, ry_send, rel_recv, ry_recv, rz_sem, a_sem, ring_send, ring_r, ring_l,
    ag_send, agz_recv, agx_recv, agy_recv, agd_recv, s_send, s_recv,
):
    ng = nz // gz
    blk = ny * ROWS
    half = nz // 2
    z, y, c, x = (lax.axis_index(n) for n in ("z", "y", "c", "x"))
    me = nz - 1
    other = 1 - c
    sgn = 1 - 2 * c
    partner = {"c": other}
    quad, zi = z // gz, lax.rem(z, gz)
    my8 = pl.ds(pl.multiple_of(8 * c, 8), 8)
    its8 = pl.ds(pl.multiple_of(8 * other, 8), 8)

    def zpos(off):
        return lax.rem(z + off + nz, nz)

    def ypos(dy):
        return lax.rem(y + dy + ny, ny)

    def send(src, dst, s, r, dev):
        pltpu.make_async_remote_copy(src, dst, s, r, device_id=dev, device_id_type=MESH).start()

    def await_bytes(ref, sem):
        pltpu.make_async_copy(ref, ref, sem).wait()

    xc_peers = [(dx, dc) for dx in range(nx) for dc in range(2) if dx or dc]

    def xc_dev(dx, dc):
        return {"x": lax.rem(x + dx, nx), "c": lax.rem(c + dc, 2)}

    def load(src, dst, i):
        pltpu.make_async_copy(src, dst, in_sem.at[i]).start()

    def loaded(dst, i):
        await_bytes(dst, in_sem.at[i])

    quads = [offset_of(r, ng) for r in range(ng)] if ng > 1 else [0]

    def quad_of(g):
        return lax.rem(quad + quads[g] + ng, ng)

    load(k_hbm, ks, 0)
    for g in range(ng):
        src = x_hbm.at[:, pl.ds(pl.multiple_of(quad_of(g) * (gz * blk), gz * blk), gz * blk)]
        pltpu.make_async_copy(src, xs.at[g], x_sem.at[g]).start()
    load(w_hbm, wv, 1)
    load(m_hbm, mv, 2)
    load(lr_hbm.at[0], lrv.at[c], 3)
    load(rr_hbm, rrv, 4)
    load(ls_hbm.at[0], lsv, 5)
    load(rs_hbm, rsv, 6)

    bar = pltpu.get_barrier_semaphore()
    for dx, dc in xc_peers:
        pl.semaphore_signal(bar, inc=1, device_id=xc_dev(dx, dc), device_id_type=MESH)

    @pl.loop(1, ny)
    def _(dy):
        pl.semaphore_signal(bar, inc=1, device_id={"y": ypos(dy)}, device_id_type=MESH)

    @pl.loop(1, nz)
    def _(dz):
        pl.semaphore_signal(bar, inc=1, device_id={"z": lax.rem(z + dz, nz)}, device_id_type=MESH)

    def matmul(g):
        await_bytes(xs.at[g], x_sem.at[g])
        out = jnp.dot(kt[...], xs[g], preferred_element_type=F32)
        for i in range(gz):
            for h in range(2):
                pt[g, h, i] = out[h * H:(h + 1) * H, i * blk:(i + 1) * blk]

    def exchange(g):
        send(pt.at[g, other], px.at[g], d_send.at[0], d_recv.at[g], partner)

    def span(g):
        return pl.ds(g * gz, gz)

    def scatter_y(g):
        await_bytes(px.at[g], d_recv.at[g])
        for i in range(gz):
            r = g * gz + i
            t = (pt[g, c, i] + px[g, i]).T.reshape(ny, ROWS, H)
            sf[r] = t
            ysend[:, r] = t.astype(BF16)
        for dst, via, slot in ((ypos(4), 2 * sgn, 2), (ypos(3), 1, 0), (ypos(-3), -1, 1)):
            send(ysend.at[dst, span(g)], yrel.at[slot, span(g)], ry_send.at[0], rel_recv.at[g], {"y": ypos(via)})
        for d, slot in ((1, 0), (-1, 1)):
            send(ysend.at[ypos(d), span(g)], yrecv.at[slot, span(g)], ry_send.at[1], ry_recv.at[g], {"y": ypos(d)})

    loaded(ks, 0)
    kt[...] = ks[...].T
    matmul(0)
    loaded(wv, 1)
    loaded(mv, 2)
    base = 0.9 * wv[...] - 0.225 * mv[...]
    ascr[0] = base[:, :H]
    ascr[1] = base[:, H:]
    afull[c, me, y, my8] = ascr[c]
    loaded(lrv.at[c], 3)

    pl.semaphore_wait(bar, (ny - 1) + (nz - 1) + len(xc_peers))

    exchange(0)
    send(ascr.at[other], afull.at[other, me, y, my8], d_send.at[1], d_recv.at[ng], partner)
    send(lrv.at[c], lrv.at[c], d_send.at[2], d_recv.at[ng + 1], partner)
    for g in range(1, ng):
        matmul(g)
        exchange(g)
        scatter_y(g - 1)
        if g == 1:
            await_bytes(ascr.at[0], d_recv.at[ng])

            @pl.loop(1, ny)
            def _(dy):
                send(afull.at[c, me, y], afull.at[c, me, y], a_sem.at[0], a_sem.at[1], {"y": ypos(dy)})
    scatter_y(ng - 1)
    if ng == 1:
        await_bytes(ascr.at[0], d_recv.at[ng])

        @pl.loop(1, ny)
        def _(dy):
            send(afull.at[c, me, y], afull.at[c, me, y], a_sem.at[0], a_sem.at[1], {"y": ypos(dy)})

    def ring_step(k):
        if k == 1:
            await_bytes(afull.at[c, me, pl.ds(0, ny - 1)], a_sem.at[1])
        else:
            await_bytes(afull.at[c, 0], ring_r.at[k - 2])
            if k <= half:
                await_bytes(afull.at[c, 0], ring_l.at[k - 2])
        if k <= half:
            src, dst = place_of(-(k - 1), nz), place_of(-k, nz)
            send(afull.at[c, src], afull.at[c, dst], ring_send.at[0], ring_r.at[k - 1], {"z": zpos(1)})
        if k < half:
            src, dst = place_of(k - 1, nz), place_of(k, nz)
            send(afull.at[c, src], afull.at[c, dst], ring_send.at[1], ring_l.at[k - 1], {"z": zpos(-1)})
        if k == half + 1:
            send(afull.at[c], afull.at[c], d_send.at[3], d_recv.at[ng + 2], partner)

    steps = iter(range(1, half + 2))

    def ring(n=1):
        for _ in range(n):
            k = next(steps, None)
            if k is not None:
                ring_step(k)

    up_mask = (1 - c).astype(F32)
    down_mask = c.astype(F32)
    for g in range(ng):
        await_bytes(yrel.at[:, span(g)], rel_recv.at[g])
        for i in range(gz):
            r = g * gz + i
            far = yrel[2, r].astype(F32)
            ysum[0, r] = (sf[r, ypos(2)] + yrel[0, r].astype(F32) + up_mask * far).astype(BF16)
            ysum[1, r] = (sf[r, ypos(-2)] + yrel[1, r].astype(F32) + down_mask * far).astype(BF16)
        for d, slot in ((2, 0), (-2, 1)):
            send(ysum.at[slot, span(g)], yrecv.at[2 + slot, span(g)], ry_send.at[2], ry_recv.at[g], {"y": ypos(d)})
        if g == ng // 2:
            ring()
    for g in range(ng):
        await_bytes(yrecv.at[:, span(g)], ry_recv.at[g])
        for i in range(gz):
            r = g * gz + i
            t = sf[r, y]
            for j in range(4):
                t = t + yrecv[j, r].astype(F32)
            zsend[r] = t
        for i in range(gz):
            if quads[g]:
                send(zsend.at[g * gz + i], zrecv.at[z], rz_sem.at[0], rz_sem.at[1], {"z": quad_of(g) * gz + i})
            elif i:
                at = lax.rem(zi + i, gz)
                send(zsend.at[g * gz + at], zrecv.at[z], rz_sem.at[0], rz_sem.at[1], {"z": quad * gz + at})
        if g == ng // 2:
            ring()
    zrecv[z] = zsend[(ng - 1) * gz + zi]
    ring()

    await_bytes(zrecv.at[pl.ds(0, nz - 1)], rz_sem.at[1])
    grad = zrecv[0]
    for r in range(1, nz):
        grad = grad + zrecv[r]
    sv[0:1] = jnp.sum(grad * grad, axis=0, keepdims=True)
    gfull[c, me, y] = grad.astype(BF16)

    groups = [(me, 1)] + [(r, 2) for r in range(nz - 3, 0, -2)] + [(0, 1)]
    ngr = len(groups)
    lag = min(3, ngr - 1)

    def gather_start(full, p):
        for r in range(nz - 1):
            off = offset_of(r, nz)
            back = place_of(-off, nz)
            j = [q for q, (r0, n) in enumerate(groups) if r0 <= back < r0 + n][0]
            send(full.at[c, me, y], full.at[c, back, y], ag_send.at[p, 0], agz_recv.at[p, j], {"z": zpos(off)})
        gather_forward(full, p, 0)

    def gather_forward(full, p, j):
        r0, n = groups[j]
        if j:
            await_bytes(full.at[c, pl.ds(r0, n), y], agz_recv.at[p, j])
        slab = full.at[c, pl.ds(r0, n), y]
        for d in (2, -2):
            send(slab, slab, ag_send.at[p, 1], agx_recv.at[p, j], {"y": ypos(d)})
        for d in (1, -1):
            send(slab, slab, ag_send.at[p, 1], agy_recv.at[p, j], {"y": ypos(d)})

    def gather_relay(full, p, j):
        r0, n = groups[j]
        await_bytes(full.at[c, pl.ds(r0, n), pl.ds(0, 2)], agx_recv.at[p, j])
        for origin, to in ((-2 * sgn, 2 * sgn), (-2, 1), (2, -1)):
            slab = full.at[c, pl.ds(r0, n), ypos(origin)]
            send(slab, slab, ag_send.at[p, 1], agy_recv.at[p, j], {"y": ypos(to)})

    def gather_land(full, p, j):
        r0, n = groups[j]
        await_bytes(full.at[c, pl.ds(r0, n), pl.ds(0, 5)], agy_recv.at[p, j])
        slab = full.at[c, pl.ds(r0, n)]
        send(slab, slab, ag_send.at[p, 2], agd_recv.at[p, j], partner)

    def gather(full, p, after_forward, before_land, after_land):
        for j in range(1, ngr):
            gather_forward(full, p, j)
            after_forward(j)
            if j >= lag:
                gather_relay(full, p, j - lag)
        for j in range(ngr - lag, ngr):
            gather_relay(full, p, j)
        before_land()
        for j in range(ngr):
            gather_land(full, p, j)
            after_land(j)

    def gather_close(full, p):
        await_bytes(full.at[0, pl.ds(0, nz - 1), 0], ag_send.at[p, 0])
        await_bytes(full.at[0, :, pl.ds(0, ny - 1)], ag_send.at[p, 1])
        await_bytes(full.at[0], ag_send.at[p, 2])

    def keep(h, j):
        r0, n = groups[j]
        for r in range(r0, r0 + n):
            gabs[h, pl.ds(pl.multiple_of(zpos(offset_of(r, nz)) * blk, blk), blk)] = gfull[h, r].reshape(blk, H)

    gather_start(gfull, 0)
    gather(gfull, 0, lambda j: ring() if j == ngr // 2 else None, ring, lambda j: keep(c, j))

    await_bytes(lrv.at[0], d_recv.at[ng + 1])
    loaded(rrv, 4)
    lm = jnp.concatenate([lrv[0].astype(F32), lrv[1].astype(F32)], axis=0).astype(BF16)
    left = jnp.dot(lm, gabs[c], preferred_element_type=F32)
    hi = left.astype(BF16)
    lo = (left - hi.astype(F32)).astype(BF16)
    rr = rrv[c]
    pre = jnp.dot(hi, rr, preferred_element_type=F32) + jnp.dot(lo, rr, preferred_element_type=F32)
    pfull[c, me, y] = pre.astype(BF16)
    gather_start(pfull, 1)
    sv[1:2] = jnp.sum(pre * pre, axis=0, keepdims=True)
    tile[...] = pre

    s1[x * 2 + c] = sv[...]
    for dx, dc in xc_peers:
        send(sv, s1.at[x * 2 + c], s_send.at[0], s_recv.at[0], xc_dev(dx, dc))
    send(tile.at[its8], own8.at[c], d_send.at[4], d_recv.at[ng + 3], partner)
    own8[c] = tile[my8]

    def total(buf, n):
        tot = buf[0]
        for i in range(1, n):
            tot = tot + buf[i]
        return tot

    def after_forward(j):
        if j == 1:
            await_bytes(s1.at[pl.ds(0, 2 * nx - 1)], s_recv.at[0])
            s2[z] = total(s1, 2 * nx)

            @pl.loop(1, nz)
            def _(dz):
                send(s2.at[z], s2.at[z], s_send.at[1], s_recv.at[1], {"z": lax.rem(z + dz, nz)})
        if j == ngr // 2:
            ring()

    def before_land():
        await_bytes(s2.at[pl.ds(0, nz - 1)], s_recv.at[1])
        s3[y] = total(s2, nz)

        @pl.loop(1, ny)
        def _(dy):
            send(s3.at[y], s3.at[y], s_send.at[2], s_recv.at[2], {"y": ypos(dy)})
        ring(half)

        for j in range(ngr):
            r0, n = groups[j]
            await_bytes(gfull.at[other, pl.ds(r0, n)], agd_recv.at[0, j])
            keep(other, j)
        gram = None
        for h in range(2):
            gown[...] = gfull[h, me, y].astype(F32)
            part = lax.dot_general(
                gown[my8].astype(BF16), gabs[h], (((1,), (1,)), ((), ())), preferred_element_type=F32
            )
            gram = part if gram is None else gram + part
        loaded(lsv, 5)
        lnv[...] = 0.95 * lsv[...] + 0.05 * gram
        loaded(rsv, 6)
        for h in range(2):
            gh = gabs[h]
            hg = lax.dot_general(gh, gh, (((0,), (0,)), ((), ())), preferred_element_type=F32)
            rnv[h] = 0.95 * rsv[h] + 0.05 * hg

    gather(pfull, 1, after_forward, before_land, lambda j: None)

    await_bytes(s3.at[pl.ds(0, ny - 1)], s_recv.at[2])
    tot = total(s3, ny)
    gs = jnp.sum(tot[0:1], axis=1, keepdims=True)
    ps = jnp.sum(tot[1:2], axis=1, keepdims=True)
    scale = jnp.sqrt(gs / (ps + 1e-06))

    await_bytes(own8.at[0], d_recv.at[ng + 3])
    wide = jnp.concatenate([own8[0], own8[1]], axis=1)
    mom = 0.9 * mv[...] + scale * wide
    upd = -0.25 * (mom + 0.4 * wv[...])
    momv[...] = mom
    upv[...] = upd
    wnv[...] = wv[...] + upd

    await_bytes(afull.at[other], d_recv.at[ng + 2])
    quarter = 0.25 * scale
    for j in range(ngr):
        r0, n = groups[j]
        await_bytes(pfull.at[other, pl.ds(r0, n)], agd_recv.at[1, j])
        for r in range(r0, r0 + n):
            rows = pl.ds(pl.multiple_of(zpos(offset_of(r, nz)) * blk, blk), blk)
            for h in range(2):
                v = afull[h, r].reshape(blk, H) - quarter * pfull[h, r].reshape(blk, H).astype(F32)
                outv[rows, h * H:(h + 1) * H] = v.astype(BF16)

    await_bytes(pt.at[:, 0], d_send.at[0])
    await_bytes(ascr.at[0], d_send.at[1])
    await_bytes(lrv.at[0], d_send.at[2])
    await_bytes(afull.at[0], d_send.at[3])
    await_bytes(own8.at[0], d_send.at[4])
    await_bytes(yrel, ry_send.at[0])
    await_bytes(ysum, ry_send.at[1])
    await_bytes(ysum, ry_send.at[2])
    await_bytes(zrecv.at[pl.ds(0, nz - 1)], rz_sem.at[0])
    await_bytes(afull.at[0, 0, pl.ds(0, ny - 1)], a_sem.at[0])
    await_bytes(afull.at[0, pl.ds(0, half)], ring_send.at[0])
    if half > 1:
        await_bytes(afull.at[0, pl.ds(0, half - 1)], ring_send.at[1])
    gather_close(gfull, 0)
    gather_close(pfull, 1)
    await_bytes(s1.at[pl.ds(0, 2 * nx - 1)], s_send.at[0])
    await_bytes(s2.at[pl.ds(0, nz - 1)], s_send.at[1])
    await_bytes(s3.at[pl.ds(0, ny - 1)], s_send.at[2])


def write_out(*refs):
    n = (len(refs) - 1) // 2
    sems = refs[-1]
    copies = [pltpu.make_async_copy(refs[i], refs[n + i], sems.at[i]) for i in range(n)]
    for copy in copies:
        copy.start()
    for copy in copies:
        copy.wait()


def body(nz, ny, nx, gz, inputs, key_grads, weights, momentum, left_stat, right_stat, left_root, right_root):
    tokens, width = inputs.shape
    ng, blk, ngr = nz // gz, ny * ROWS, nz // 2 + 1
    dma = pltpu.SemaphoreType.DMA
    v = pltpu.VMEM
    scratch = [
        v((ng, tokens, gz * blk), BF16), v((tokens, 2 * H), BF16), v((2 * H, tokens), BF16),
        v((ng, 2, gz, H, blk), F32), v((ng, gz, H, blk), F32),
        v((nz, ny, ROWS, H), F32), v((ny, nz, ROWS, H), BF16),
        v((3, nz, ROWS, H), BF16), v((2, nz, ROWS, H), BF16), v((4, nz, ROWS, H), BF16),
        v((nz, ROWS, H), F32), v((nz, ROWS, H), F32),
        v((2, nz, ny, ROWS, H), BF16), v((2, width, H), BF16), v((2, nz, ny, ROWS, H), BF16), v((2, nz, ny, ROWS, H), F32),
        v((2, 8, H), F32), v((ROWS, H), F32), v((2, 8, H), F32), v((ROWS, H), F32),
        v((8, 2 * H), F32), v((8, 2 * H), F32), v((8, width), F32), v((2, H, H), F32), v((2, 8, width), BF16), v((2, H, H), BF16),
        v((2, H), F32), v((2 * nx, 2, H), F32), v((nz, 2, H), F32), v((ny, 2, H), F32),
        dma((7,)), dma((ng,)), dma((5,)), dma((ng + 4,)), dma((3,)), dma((ng,)), dma((ng,)), dma((2,)), dma((2,)),
        dma((2,)), dma((nz // 2,)), dma((nz // 2,)),
        dma((2, 3)), dma((2, ngr)), dma((2, ngr)), dma((2, ngr)), dma((2, ngr)), dma((3,)), dma((3,)),
    ]
    sds = jax.ShapeDtypeStruct
    anyspace = pl.BlockSpec(memory_space=pl.ANY)
    local = pl.BlockSpec(memory_space=pltpu.VMEM)
    shapes = (
        (weights.shape, F32), ((8, width), F32), (right_stat.shape, F32),
        (weights.shape, F32), (weights.shape, F32), ((width, 2 * H), BF16),
    )
    held = pl.pallas_call(
        functools.partial(kernel, nz, ny, nx, gz),
        out_shape=tuple(HELD(*s) for s in shapes),
        in_specs=[anyspace] * 8,
        out_specs=(local,) * 6,
        scratch_shapes=scratch,
        compiler_params=pltpu.CompilerParams(collective_id=0, has_side_effects=True, vmem_limit_bytes=56 * 2**20),
    )(inputs, key_grads, weights, momentum, left_stat, right_stat, left_root, right_root)
    mom, left, right, upd, nxt, copy = pl.pallas_call(
        write_out,
        out_shape=tuple(sds(*s) for s in shapes),
        in_specs=[local] * 6,
        out_specs=(anyspace,) * 6,
        scratch_shapes=[dma((6,))],
    )(*(pltpu.with_memory_space_constraint(h, pltpu.VMEM) for h in held))
    return mom, left[None], right, upd, nxt, copy


def build(devices, nz, ny, nx, gz):
    split = Mesh(devices.reshape(nz, ny, 2, nx), ("z", "y", "c", "x"))
    fs = ("z", "y", "c")
    in_specs = (
        P(fs, None), P(fs, "x"), P(fs, "x"), P(fs, "x"),
        P("x", fs, None), P("x", None, None), P("x", fs, None), P("x", None, None),
    )
    out_specs = (P(fs, "x"), P("x", fs, None), P("x", None, None), P(fs, "x"), P(fs, "x"), P(None, "x"))
    return jax.shard_map(
        functools.partial(body, nz, ny, nx, gz), mesh=split, in_specs=in_specs, out_specs=out_specs, check_vma=False
    )


def solution(mesh):
    return build(mesh.devices, 16, 8, mesh.shape["tp"], 4)
```

time: 96.7 us -> 90.8 us (0.939)
  local copies, waits for them, and re-layouts: 9.19 us -> 0 us
  Pallas kernels: 86.4 us -> 90 us
    unnamed x6 -> x0, local copies, waits for them, and re-layouts: 9.19 us -> none
    pallas_call x1 -> x2, Pallas kernels: 86.4 us -> 90 us  [the longest x1 88.9 us: body(): pl.pallas_call(functools.partial(kernel, nz, ny, nx, gz), out_shape=tuple...]
where the time goes in v2:
time: 90.8 us; the launch traced here: 90.6 us
  Pallas kernels  90 us (99%)
    pallas_call x1, Pallas kernels, body(): pl.pallas_call(functools.partial(kernel, nz, ny, nx, gz), out_shape=tuple...  88.9 us

profile of v2, /device:TPU:1, one launch (start us, length us, event | category | flops | bytes accessed | tf_op | source)
XLA Modules:
  0.0 90.6 jit_solution(474288758986706114)
XLA Ops:
  0.6 88.9 %shard_map.127 = (f32[8,256]{1,0:T(8,128)S(1)}, f32[8,2048]{1,0:T(8,128)S(1)}, f32[2,128,128]{2,1,0:T(8,128)S(1)}, f32[8,256]{1,0:T(8,128)S(1)}, f32[8,256]{1,0:T(8,128)S(1)}, /*index=5*/bf16[2048,256]{1,0:T(8,128)(2,1)S(1)}) custom-call(bf16[2048,2048]{1,0:T(8,128)(2,1)} %x_hbm.1, bf16[2048,256]{1,0:T(8,128)(2,1)} %k_hbm.1, f32[8,256]{1,0:T(8,128)} %w_hbm.1, ...), custom_call_target="tpu_custom_call" | custom-call | tf_op jit(solution)/shard_map/pallas_call | solution.py:440
  89.5 1.1 %shard_map.128 = (f32[8,256]{1,0:T(8,128)}, f32[8,2048]{1,0:T(8,128)}, f32[2,128,128]{2,1,0:T(8,128)}, f32[8,256]{1,0:T(8,128)}, f32[8,256]{1,0:T(8,128)}, /*index=5*/bf16[2048,256]{1,0:T(8,128)(2,1)}) custom-call(f32[8,256]{1,0:T(8,128)S(1)} %get-tuple-element.18.refs_0_, f32[8,2048]{1,0:T(8,128)S(1)} %get-tuple-element.19.refs_1_, ...), custom_call_target="tpu_custom_call" | custom-call | tf_op jit(solution)/shard_map/pallas_call | solution.py:448

commit v3 on v2

--- a/solution.py
+++ b/solution.py
@@ -41,7 +41,7 @@
     xs, ks, kt, pt, px, sf, ysend, yrel, ysum, yrecv, zsend, zrecv, gfull, gabs, pfull, afull, ascr, tile, own8, gown,
     wv, mv, lsv, rsv, lrv, rrv,
     sv, s1, s2, s3,
-    in_sem, x_sem, d_send, d_recv, ry_send, rel_recv, ry_recv, rz_sem, a_sem, ring_send, ring_r, ring_l,
+    hello, in_sem, x_sem, d_send, d_recv, ry_send, rel_recv, ry_recv, rz_sem, a_send, a_recv,
     ag_send, agz_recv, agx_recv, agy_recv, agd_recv, s_send, s_recv,
 ):
     ng = nz // gz
@@ -103,8 +103,8 @@
     def _(dy):
         pl.semaphore_signal(bar, inc=1, device_id={"y": ypos(dy)}, device_id_type=MESH)
 
-    @pl.loop(1, nz)
-    def _(dz):
+    near = sorted({d % nz for d in range(-4, 5) if d % nz})
+    for dz in near:
         pl.semaphore_signal(bar, inc=1, device_id={"z": lax.rem(z + dz, nz)}, device_id_type=MESH)
 
     def matmul(g):
@@ -143,56 +143,19 @@
     afull[c, me, y, my8] = ascr[c]
     loaded(lrv.at[c], 3)
 
-    pl.semaphore_wait(bar, (ny - 1) + (nz - 1) + len(xc_peers))
+    pl.semaphore_wait(bar, (ny - 1) + len(near) + len(xc_peers))
+    far = len(near) < nz - 1
+    if far:
+        for dz in (4, -4):
+            pl.semaphore_signal(hello, inc=1, device_id={"z": zpos(dz)}, device_id_type=MESH)
 
     exchange(0)
     send(ascr.at[other], afull.at[other, me, y, my8], d_send.at[1], d_recv.at[ng], partner)
     send(lrv.at[c], lrv.at[c], d_send.at[2], d_recv.at[ng + 1], partner)
-    for g in range(1, ng):
-        matmul(g)
-        exchange(g)
-        scatter_y(g - 1)
-        if g == 1:
-            await_bytes(ascr.at[0], d_recv.at[ng])
-
-            @pl.loop(1, ny)
-            def _(dy):
-                send(afull.at[c, me, y], afull.at[c, me, y], a_sem.at[0], a_sem.at[1], {"y": ypos(dy)})
-    scatter_y(ng - 1)
-    if ng == 1:
-        await_bytes(ascr.at[0], d_recv.at[ng])
-
-        @pl.loop(1, ny)
-        def _(dy):
-            send(afull.at[c, me, y], afull.at[c, me, y], a_sem.at[0], a_sem.at[1], {"y": ypos(dy)})
-
-    def ring_step(k):
-        if k == 1:
-            await_bytes(afull.at[c, me, pl.ds(0, ny - 1)], a_sem.at[1])
-        else:
-            await_bytes(afull.at[c, 0], ring_r.at[k - 2])
-            if k <= half:
-                await_bytes(afull.at[c, 0], ring_l.at[k - 2])
-        if k <= half:
-            src, dst = place_of(-(k - 1), nz), place_of(-k, nz)
-            send(afull.at[c, src], afull.at[c, dst], ring_send.at[0], ring_r.at[k - 1], {"z": zpos(1)})
-        if k < half:
-            src, dst = place_of(k - 1, nz), place_of(k, nz)
-            send(afull.at[c, src], afull.at[c, dst], ring_send.at[1], ring_l.at[k - 1], {"z": zpos(-1)})
-        if k == half + 1:
-            send(afull.at[c], afull.at[c], d_send.at[3], d_recv.at[ng + 2], partner)
-
-    steps = iter(range(1, half + 2))
-
-    def ring(n=1):
-        for _ in range(n):
-            k = next(steps, None)
-            if k is not None:
-                ring_step(k)
-
     up_mask = (1 - c).astype(F32)
     down_mask = c.astype(F32)
-    for g in range(ng):
+
+    def relay_y(g):
         await_bytes(yrel.at[:, span(g)], rel_recv.at[g])
         for i in range(gz):
             r = g * gz + i
@@ -201,9 +164,8 @@
             ysum[1, r] = (sf[r, ypos(-2)] + yrel[1, r].astype(F32) + down_mask * far).astype(BF16)
         for d, slot in ((2, 0), (-2, 1)):
             send(ysum.at[slot, span(g)], yrecv.at[2 + slot, span(g)], ry_send.at[2], ry_recv.at[g], {"y": ypos(d)})
-        if g == ng // 2:
-            ring()
-    for g in range(ng):
+
+    def scatter_z(g):
         await_bytes(yrecv.at[:, span(g)], ry_recv.at[g])
         for i in range(gz):
             r = g * gz + i
@@ -217,10 +179,66 @@
             elif i:
                 at = lax.rem(zi + i, gz)
                 send(zsend.at[g * gz + at], zrecv.at[z], rz_sem.at[0], rz_sem.at[1], {"z": quad * gz + at})
-        if g == ng // 2:
-            ring()
+
+    pieces = ((0, half), (half, nz - half))
+
+    def base_z(is_near):
+        if is_near:
+            await_bytes(ascr.at[0], d_recv.at[ng])
+        elif far:
+            pl.semaphore_wait(hello, 2)
+        for r in range(nz - 1):
+            off = offset_of(r, nz)
+            if (off % nz in near) != is_near:
+                continue
+            send(afull.at[c, me, y], afull.at[c, place_of(-off, nz), y], a_send.at[0], a_recv.at[0], {"z": zpos(off)})
+
+    def base_y(p):
+        r0, n = pieces[p]
+        if p == 0:
+            await_bytes(afull.at[c, pl.ds(0, nz - 1), y], a_recv.at[0])
+        slab = afull.at[c, pl.ds(r0, n), y]
+        for d in (2, -2):
+            send(slab, slab, a_send.at[1], a_recv.at[1 + p], {"y": ypos(d)})
+        for d in (1, -1):
+            send(slab, slab, a_send.at[1], a_recv.at[3 + p], {"y": ypos(d)})
+
+    def base_relay(p):
+        r0, n = pieces[p]
+        await_bytes(afull.at[c, pl.ds(r0, n), pl.ds(0, 2)], a_recv.at[1 + p])
+        for origin, to in ((-2 * sgn, 2 * sgn), (-2, 1), (2, -1)):
+            slab = afull.at[c, pl.ds(r0, n), ypos(origin)]
+            send(slab, slab, a_send.at[1], a_recv.at[3 + p], {"y": ypos(to)})
+
+    def base_land(p):
+        r0, n = pieces[p]
+        await_bytes(afull.at[c, pl.ds(r0, n), pl.ds(0, 5)], a_recv.at[3 + p])
+        slab = afull.at[c, pl.ds(r0, n)]
+        send(slab, slab, d_send.at[3], a_recv.at[5 + p], partner)
+
+    for g in range(1, ng):
+        matmul(g)
+        exchange(g)
+        scatter_y(g - 1)
+        if g == 1:
+            base_z(True)
+    if ng == 1:
+        base_z(True)
+    base_z(False)
+    early = min(2, ng - 1)
+    if early:
+        relay_y(0)
+    scatter_y(ng - 1)
+    for g in range(1 if early else 0, ng - 1):
+        relay_y(g)
+    if ng > 1:
+        scatter_z(0)
+    relay_y(ng - 1)
+    for g in range(1 if ng > 1 else 0, ng):
+        scatter_z(g)
     zrecv[z] = zsend[(ng - 1) * gz + zi]
-    ring()
+    base_y(0)
+    base_y(1)
 
     await_bytes(zrecv.at[pl.ds(0, nz - 1)], rz_sem.at[1])
     grad = zrecv[0]
@@ -231,10 +249,12 @@
 
     groups = [(me, 1)] + [(r, 2) for r in range(nz - 3, 0, -2)] + [(0, 1)]
     ngr = len(groups)
-    lag = min(3, ngr - 1)
+    lag = min(5, ngr - 1)
+    direct = range(max(ngr - 2, 1), ngr)
 
     def gather_start(full, p):
-        for r in range(nz - 1):
+        order = [0, 1, 2, 13, 14, 3, 4, 11, 12, 5, 6, 9, 10, 7, 8] if nz == 16 else range(nz - 1)
+        for r in order:
             off = offset_of(r, nz)
             back = place_of(-off, nz)
             j = [q for q, (r0, n) in enumerate(groups) if r0 <= back < r0 + n][0]
@@ -246,12 +266,18 @@
         if j:
             await_bytes(full.at[c, pl.ds(r0, n), y], agz_recv.at[p, j])
         slab = full.at[c, pl.ds(r0, n), y]
+        if j in direct:
+            for d in (4, 3, -3, 2, -2, 1, -1):
+                send(slab, slab, ag_send.at[p, 1], agy_recv.at[p, j], {"y": ypos(d)})
+            return
         for d in (2, -2):
             send(slab, slab, ag_send.at[p, 1], agx_recv.at[p, j], {"y": ypos(d)})
         for d in (1, -1):
             send(slab, slab, ag_send.at[p, 1], agy_recv.at[p, j], {"y": ypos(d)})
 
     def gather_relay(full, p, j):
+        if j in direct:
+            return
         r0, n = groups[j]
         await_bytes(full.at[c, pl.ds(r0, n), pl.ds(0, 2)], agx_recv.at[p, j])
         for origin, to in ((-2 * sgn, 2 * sgn), (-2, 1), (2, -1)):
@@ -260,7 +286,7 @@
 
     def gather_land(full, p, j):
         r0, n = groups[j]
-        await_bytes(full.at[c, pl.ds(r0, n), pl.ds(0, 5)], agy_recv.at[p, j])
+        await_bytes(full.at[c, pl.ds(r0, n), pl.ds(0, ny - 1 if j in direct else 5)], agy_recv.at[p, j])
         slab = full.at[c, pl.ds(r0, n)]
         send(slab, slab, ag_send.at[p, 2], agd_recv.at[p, j], partner)
 
@@ -288,7 +314,7 @@
             gabs[h, pl.ds(pl.multiple_of(zpos(offset_of(r, nz)) * blk, blk), blk)] = gfull[h, r].reshape(blk, H)
 
     gather_start(gfull, 0)
-    gather(gfull, 0, lambda j: ring() if j == ngr // 2 else None, ring, lambda j: keep(c, j))
+    gather(gfull, 0, lambda j: None, lambda: None, lambda j: keep(c, j))
 
     await_bytes(lrv.at[0], d_recv.at[ng + 1])
     loaded(rrv, 4)
@@ -300,12 +326,17 @@
     pre = jnp.dot(hi, rr, preferred_element_type=F32) + jnp.dot(lo, rr, preferred_element_type=F32)
     pfull[c, me, y] = pre.astype(BF16)
     gather_start(pfull, 1)
+    for p in range(2):
+        base_relay(p)
     sv[1:2] = jnp.sum(pre * pre, axis=0, keepdims=True)
     tile[...] = pre
 
-    s1[x * 2 + c] = sv[...]
-    for dx, dc in xc_peers:
-        send(sv, s1.at[x * 2 + c], s_send.at[0], s_recv.at[0], xc_dev(dx, dc))
+    s2[z] = sv[...]
+
+    @pl.loop(1, nz)
+    def _(dz):
+        send(sv, s2.at[z], s_send.at[1], s_recv.at[1], {"z": lax.rem(z + dz, nz)})
+
     send(tile.at[its8], own8.at[c], d_send.at[4], d_recv.at[ng + 3], partner)
     own8[c] = tile[my8]
 
@@ -316,25 +347,15 @@
         return tot
 
     def after_forward(j):
-        if j == 1:
-            await_bytes(s1.at[pl.ds(0, 2 * nx - 1)], s_recv.at[0])
-            s2[z] = total(s1, 2 * nx)
-
-            @pl.loop(1, nz)
-            def _(dz):
-                send(s2.at[z], s2.at[z], s_send.at[1], s_recv.at[1], {"z": lax.rem(z + dz, nz)})
-        if j == ngr // 2:
-            ring()
+        if j == ngr - 1:
+            await_bytes(s2.at[pl.ds(0, nz - 1)], s_recv.at[1])
+            s3[y] = total(s2, nz)
+
+            @pl.loop(1, ny)
+            def _(dy):
+                send(s3.at[y], s3.at[y], s_send.at[2], s_recv.at[2], {"y": ypos(dy)})
 
     def before_land():
-        await_bytes(s2.at[pl.ds(0, nz - 1)], s_recv.at[1])
-        s3[y] = total(s2, nz)
-
-        @pl.loop(1, ny)
-        def _(dy):
-            send(s3.at[y], s3.at[y], s_send.at[2], s_recv.at[2], {"y": ypos(dy)})
-        ring(half)
-
         for j in range(ngr):
             r0, n = groups[j]
             await_bytes(gfull.at[other, pl.ds(r0, n)], agd_recv.at[0, j])
@@ -353,11 +374,17 @@
             gh = gabs[h]
             hg = lax.dot_general(gh, gh, (((0,), (0,)), ((), ())), preferred_element_type=F32)
             rnv[h] = 0.95 * rsv[h] + 0.05 * hg
+        for p in range(2):
+            base_land(p)
+        await_bytes(s3.at[pl.ds(0, ny - 1)], s_recv.at[2])
+        s1[x * 2 + c] = total(s3, ny)
+        for dx, dc in xc_peers:
+            send(s1.at[x * 2 + c], s1.at[x * 2 + c], s_send.at[0], s_recv.at[0], xc_dev(dx, dc))
 
     gather(pfull, 1, after_forward, before_land, lambda j: None)
 
-    await_bytes(s3.at[pl.ds(0, ny - 1)], s_recv.at[2])
-    tot = total(s3, ny)
+    await_bytes(s1.at[pl.ds(0, 2 * nx - 1)], s_recv.at[0])
+    tot = total(s1, 2 * nx)
     gs = jnp.sum(tot[0:1], axis=1, keepdims=True)
     ps = jnp.sum(tot[1:2], axis=1, keepdims=True)
     scale = jnp.sqrt(gs / (ps + 1e-06))
@@ -370,7 +397,8 @@
     upv[...] = upd
     wnv[...] = wv[...] + upd
 
-    await_bytes(afull.at[other], d_recv.at[ng + 2])
+    for p in range(2):
+        await_bytes(afull.at[other, pl.ds(*pieces[p])], a_recv.at[5 + p])
     quarter = 0.25 * scale
     for j in range(ngr):
         r0, n = groups[j]
@@ -390,10 +418,8 @@
     await_bytes(ysum, ry_send.at[1])
     await_bytes(ysum, ry_send.at[2])
     await_bytes(zrecv.at[pl.ds(0, nz - 1)], rz_sem.at[0])
-    await_bytes(afull.at[0, 0, pl.ds(0, ny - 1)], a_sem.at[0])
-    await_bytes(afull.at[0, pl.ds(0, half)], ring_send.at[0])
-    if half > 1:
-        await_bytes(afull.at[0, pl.ds(0, half - 1)], ring_send.at[1])
+    await_bytes(afull.at[0, pl.ds(0, nz - 1), 0], a_send.at[0])
+    await_bytes(afull.at[0, :, pl.ds(0, ny - 1)], a_send.at[1])
     gather_close(gfull, 0)
     gather_close(pfull, 1)
     await_bytes(s1.at[pl.ds(0, 2 * nx - 1)], s_send.at[0])
@@ -426,8 +452,7 @@
         v((2, 8, H), F32), v((ROWS, H), F32), v((2, 8, H), F32), v((ROWS, H), F32),
         v((8, 2 * H), F32), v((8, 2 * H), F32), v((8, width), F32), v((2, H, H), F32), v((2, 8, width), BF16), v((2, H, H), BF16),
         v((2, H), F32), v((2 * nx, 2, H), F32), v((nz, 2, H), F32), v((ny, 2, H), F32),
-        dma((7,)), dma((ng,)), dma((5,)), dma((ng + 4,)), dma((3,)), dma((ng,)), dma((ng,)), dma((2,)), dma((2,)),
-        dma((2,)), dma((nz // 2,)), dma((nz // 2,)),
+        pltpu.SemaphoreType.REGULAR, dma((7,)), dma((ng,)), dma((5,)), dma((ng + 4,)), dma((3,)), dma((ng,)), dma((ng,)), dma((2,)), dma((2,)), dma((7,)),
         dma((2, 3)), dma((2, ngr)), dma((2, ngr)), dma((2, ngr)), dma((2, ngr)), dma((3,)), dma((3,)),
     ]
     sds = jax.ShapeDtypeStruct

time: 90.8 us -> 80.9 us (0.89)
  Pallas kernels: 90 us -> 80.2 us
    pallas_call x1, Pallas kernels: 88.9 us -> 79.1 us  [body(): pl.pallas_call(functools.partial(kernel, nz, ny, nx, gz), out_shape=tuple...]
where the time goes in v3:
time: 80.9 us; the launch traced here: 80.8 us
  Pallas kernels  80.2 us (99%)
    pallas_call x1, Pallas kernels, body(): pl.pallas_call(functools.partial(kernel, nz, ny, nx, gz), out_shape=tuple...  79.1 us

profile of v3, /device:TPU:1, one launch (start us, length us, event | category | flops | bytes accessed | tf_op | source)
XLA Modules:
  0.0 80.8 jit_solution(14173602272635363962)
XLA Ops:
  0.6 79.1 %shard_map.127 = (f32[8,256]{1,0:T(8,128)S(1)}, f32[8,2048]{1,0:T(8,128)S(1)}, f32[2,128,128]{2,1,0:T(8,128)S(1)}, f32[8,256]{1,0:T(8,128)S(1)}, f32[8,256]{1,0:T(8,128)S(1)}, /*index=5*/bf16[2048,256]{1,0:T(8,128)(2,1)S(1)}) custom-call(bf16[2048,2048]{1,0:T(8,128)(2,1)} %x_hbm.1, bf16[2048,256]{1,0:T(8,128)(2,1)} %k_hbm.1, f32[8,256]{1,0:T(8,128)} %w_hbm.1, ...), custom_call_target="tpu_custom_call" | custom-call | tf_op jit(solution)/shard_map/pallas_call | solution.py:465
  79.7 1.1 %shard_map.128 = (f32[8,256]{1,0:T(8,128)}, f32[8,2048]{1,0:T(8,128)}, f32[2,128,128]{2,1,0:T(8,128)}, f32[8,256]{1,0:T(8,128)}, f32[8,256]{1,0:T(8,128)}, /*index=5*/bf16[2048,256]{1,0:T(8,128)(2,1)}) custom-call(f32[8,256]{1,0:T(8,128)S(1)} %get-tuple-element.18.refs_0_, f32[8,2048]{1,0:T(8,128)S(1)} %get-tuple-element.19.refs_1_, ...), custom_call_target="tpu_custom_call" | custom-call | tf_op jit(solution)/shard_map/pallas_call | solution.py:473

commit v4 on v3

--- a/solution.py
+++ b/solution.py
@@ -247,13 +247,13 @@
     sv[0:1] = jnp.sum(grad * grad, axis=0, keepdims=True)
     gfull[c, me, y] = grad.astype(BF16)
 
-    groups = [(me, 1)] + [(r, 2) for r in range(nz - 3, 0, -2)] + [(0, 1)]
+    groups = [(me, 1), (13, 2), (9, 4), (5, 4), (1, 4), (0, 1)] if nz == 16 else [(me, 1)] + [(r, 2) for r in range(nz - 3, 0, -2)] + [(0, 1)]
     ngr = len(groups)
-    lag = min(5, ngr - 1)
+    lag = min(3, ngr - 1)
     direct = range(max(ngr - 2, 1), ngr)
 
     def gather_start(full, p):
-        order = [0, 1, 2, 13, 14, 3, 4, 11, 12, 5, 6, 9, 10, 7, 8] if nz == 16 else range(nz - 1)
+        order = [*range(nz - 3, nz - 1), *range(nz - 3)] if nz > 2 else [0]
         for r in order:
             off = offset_of(r, nz)
             back = place_of(-off, nz)
@@ -326,17 +326,17 @@
     pre = jnp.dot(hi, rr, preferred_element_type=F32) + jnp.dot(lo, rr, preferred_element_type=F32)
     pfull[c, me, y] = pre.astype(BF16)
     gather_start(pfull, 1)
+    sv[1:2] = jnp.sum(pre * pre, axis=0, keepdims=True)
+    tile[...] = pre
+
+    s3[y] = sv[...]
+
+    @pl.loop(1, ny)
+    def _(dy):
+        send(sv, s3.at[y], s_send.at[2], s_recv.at[2], {"y": ypos(dy)})
+
     for p in range(2):
         base_relay(p)
-    sv[1:2] = jnp.sum(pre * pre, axis=0, keepdims=True)
-    tile[...] = pre
-
-    s2[z] = sv[...]
-
-    @pl.loop(1, nz)
-    def _(dz):
-        send(sv, s2.at[z], s_send.at[1], s_recv.at[1], {"z": lax.rem(z + dz, nz)})
-
     send(tile.at[its8], own8.at[c], d_send.at[4], d_recv.at[ng + 3], partner)
     own8[c] = tile[my8]
 
@@ -346,14 +346,12 @@
             tot = tot + buf[i]
         return tot
 
-    def after_forward(j):
-        if j == ngr - 1:
-            await_bytes(s2.at[pl.ds(0, nz - 1)], s_recv.at[1])
-            s3[y] = total(s2, nz)
-
-            @pl.loop(1, ny)
-            def _(dy):
-                send(s3.at[y], s3.at[y], s_send.at[2], s_recv.at[2], {"y": ypos(dy)})
+    await_bytes(s3.at[pl.ds(0, ny - 1)], s_recv.at[2])
+    s2[z] = total(s3, ny)
+
+    @pl.loop(1, nz)
+    def _(dz):
+        send(s2.at[z], s2.at[z], s_send.at[1], s_recv.at[1], {"z": lax.rem(z + dz, nz)})
 
     def before_land():
         for j in range(ngr):
@@ -376,12 +374,12 @@
             rnv[h] = 0.95 * rsv[h] + 0.05 * hg
         for p in range(2):
             base_land(p)
-        await_bytes(s3.at[pl.ds(0, ny - 1)], s_recv.at[2])
-        s1[x * 2 + c] = total(s3, ny)
+        await_bytes(s2.at[pl.ds(0, nz - 1)], s_recv.at[1])
+        s1[x * 2 + c] = total(s2, nz)
         for dx, dc in xc_peers:
             send(s1.at[x * 2 + c], s1.at[x * 2 + c], s_send.at[0], s_recv.at[0], xc_dev(dx, dc))
 
-    gather(pfull, 1, after_forward, before_land, lambda j: None)
+    gather(pfull, 1, lambda j: None, before_land, lambda j: None)
 
     await_bytes(s1.at[pl.ds(0, 2 * nx - 1)], s_recv.at[0])
     tot = total(s1, 2 * nx)

time: 80.9 us -> 76.3 us (0.943)
  Pallas kernels: 80.2 us -> 75.6 us
    pallas_call x1, Pallas kernels: 79.1 us -> 74.4 us  [body(): pl.pallas_call(functools.partial(kernel, nz, ny, nx, gz), out_shape=tuple...]
where the time goes in v4:
time: 76.3 us; the launch traced here: 76.2 us
  Pallas kernels  75.6 us (99%)
    pallas_call x1, Pallas kernels, body(): pl.pallas_call(functools.partial(kernel, nz, ny, nx, gz), out_shape=tuple...  74.4 us

profile of v4, /device:TPU:1, one launch (start us, length us, event | category | flops | bytes accessed | tf_op | source)
XLA Modules:
  0.0 76.2 jit_solution(16267871927078739252)
XLA Ops:
  0.6 74.4 %shard_map.127 = (f32[8,256]{1,0:T(8,128)S(1)}, f32[8,2048]{1,0:T(8,128)S(1)}, f32[2,128,128]{2,1,0:T(8,128)S(1)}, f32[8,256]{1,0:T(8,128)S(1)}, f32[8,256]{1,0:T(8,128)S(1)}, /*index=5*/bf16[2048,256]{1,0:T(8,128)(2,1)S(1)}) custom-call(bf16[2048,2048]{1,0:T(8,128)(2,1)} %x_hbm.1, bf16[2048,256]{1,0:T(8,128)(2,1)} %k_hbm.1, f32[8,256]{1,0:T(8,128)} %w_hbm.1, ...), custom_call_target="tpu_custom_call" | custom-call | tf_op jit(solution)/shard_map/pallas_call | solution.py:463
  75.1 1.1 %shard_map.128 = (f32[8,256]{1,0:T(8,128)}, f32[8,2048]{1,0:T(8,128)}, f32[2,128,128]{2,1,0:T(8,128)}, f32[8,256]{1,0:T(8,128)}, f32[8,256]{1,0:T(8,128)}, /*index=5*/bf16[2048,256]{1,0:T(8,128)(2,1)}) custom-call(f32[8,256]{1,0:T(8,128)S(1)} %get-tuple-element.18.refs_0_, f32[8,2048]{1,0:T(8,128)S(1)} %get-tuple-element.19.refs_1_, ...), custom_call_target="tpu_custom_call" | custom-call | tf_op jit(solution)/shard_map/pallas_call | solution.py:471

commit v5 on v4

--- a/solution.py
+++ b/solution.py
@@ -250,7 +250,7 @@
     groups = [(me, 1), (13, 2), (9, 4), (5, 4), (1, 4), (0, 1)] if nz == 16 else [(me, 1)] + [(r, 2) for r in range(nz - 3, 0, -2)] + [(0, 1)]
     ngr = len(groups)
     lag = min(3, ngr - 1)
-    direct = range(max(ngr - 2, 1), ngr)
+    direct = range(max(ngr - 1, 1), ngr)
 
     def gather_start(full, p):
         order = [*range(nz - 3, nz - 1), *range(nz - 3)] if nz > 2 else [0]

time: 76.3 us -> 77.7 us (1.018)
  Pallas kernels: 75.6 us -> 76.9 us
    pallas_call x1, Pallas kernels: 74.4 us -> 75.8 us  [body(): pl.pallas_call(functools.partial(kernel, nz, ny, nx, gz), out_shape=tuple...]
where the time goes in v5:
time: 77.7 us; the launch traced here: 77.6 us
  Pallas kernels  76.9 us (99%)
    pallas_call x1, Pallas kernels, body(): pl.pallas_call(functools.partial(kernel, nz, ny, nx, gz), out_shape=tuple...  75.8 us

profile of v5, /device:TPU:1, one launch (start us, length us, event | category | flops | bytes accessed | tf_op | source)
XLA Modules:
  0.0 77.6 jit_solution(9327038345878076427)
XLA Ops:
  0.6 75.8 %shard_map.127 = (f32[8,256]{1,0:T(8,128)S(1)}, f32[8,2048]{1,0:T(8,128)S(1)}, f32[2,128,128]{2,1,0:T(8,128)S(1)}, f32[8,256]{1,0:T(8,128)S(1)}, f32[8,256]{1,0:T(8,128)S(1)}, /*index=5*/bf16[2048,256]{1,0:T(8,128)(2,1)S(1)}) custom-call(bf16[2048,2048]{1,0:T(8,128)(2,1)} %x_hbm.1, bf16[2048,256]{1,0:T(8,128)(2,1)} %k_hbm.1, f32[8,256]{1,0:T(8,128)} %w_hbm.1, ...), custom_call_target="tpu_custom_call" | custom-call | tf_op jit(solution)/shard_map/pallas_call | solution.py:463
  76.5 1.1 %shard_map.128 = (f32[8,256]{1,0:T(8,128)}, f32[8,2048]{1,0:T(8,128)}, f32[2,128,128]{2,1,0:T(8,128)}, f32[8,256]{1,0:T(8,128)}, f32[8,256]{1,0:T(8,128)}, /*index=5*/bf16[2048,256]{1,0:T(8,128)(2,1)}) custom-call(f32[8,256]{1,0:T(8,128)S(1)} %get-tuple-element.18.refs_0_, f32[8,2048]{1,0:T(8,128)S(1)} %get-tuple-element.19.refs_1_, ...), custom_call_target="tpu_custom_call" | custom-call | tf_op jit(solution)/shard_map/pallas_call | solution.py:471
